TPU v7x, 32 devices: a whole 2x2x4 slice. The times are simulated.
32 devices in a mesh: sp: 8 (over z, x), tp: 4 (over y, core).
Axes of the slice: x: 2, y: 2, z: 4, core: 2. Of those that a mesh axis runs over, the one named last changes fastest.
Arguments:
- tokens: bfloat16 [2048, 2048], P(('sp', 'tp')), may hold values from -6 to 6
- query_weight: bfloat16 [2048, 2048], P('sp', 'tp'), may hold values from -0.125 to 0.125
- key_weight: bfloat16 [2048, 512], P('sp', 'tp'), may hold values from -0.125 to 0.125
- value_weight: bfloat16 [2048, 512], P('sp', 'tp'), may hold values from -0.125 to 0.125
- out_weight: bfloat16 [2048, 2048], P('tp', 'sp'), may hold values from -0.125 to 0.125
- query_gain: float32 [128], replicated, may hold values from 0.1 to 1.9
- key_gain: float32 [128], replicated, may hold values from 0.1 to 1.9
Outputs:
- mixed: bfloat16 [2048, 2048], P(('sp', 'tp'))
All inputs are finite; a program needn't handle non-finite values.
Results may differ from a plain program's by a relative error of at most 0.02.
Values may be sent and summed in bfloat16 or wider, within the bound.
A program may use at most 64 MiB of HBM per device.

v0:
```python
import math

import jax
import jax.numpy as jnp
from jax import lax
from jax.sharding import PartitionSpec as P

HEAD_DIM = 128
GRID_W = 64


eps = 1e-06
rope_base = 10000.0


def gathered_then(slab, axis, dim, apply):
    everything = lax.all_gather(slab, axis, axis=dim, tiled=True)
    return apply(everything, jnp.int32(0))


def over_all(shard, axis, dim, absorb, state):
    everything = jax.tree.map(lambda a: lax.all_gather(a, axis, axis=dim, tiled=True), shard)
    return absorb(state, everything, jnp.int32(0))


def summed_rows(product, rows, axis):
    everything = product(jnp.int32(0), lax.axis_size(axis) * rows)
    own = lax.psum_scatter(everything.astype(jnp.bfloat16), axis, scatter_dimension=0, tiled=True)
    return own.astype(jnp.float32)


def normalize(raw, gain):
    wide = raw.astype(jnp.float32)
    return wide * lax.rsqrt(jnp.mean(wide * wide, axis=-1, keepdims=True) + eps) * gain


def rotate(values_in, positions):
    pair_count = values_in.shape[-1] // 4
    inverse_rate = rope_base ** (
        -jnp.arange(0, 2 * pair_count, 2, dtype=jnp.float32) / (2 * pair_count)
    )
    grid_row = (positions // GRID_W).astype(jnp.float32)
    grid_column = (positions % GRID_W).astype(jnp.float32)
    angles = jnp.stack(
        [grid_row[:, None] * inverse_rate, grid_column[:, None] * inverse_rate], axis=1
    )
    cosine = jnp.cos(angles)[:, None]
    sine = jnp.sin(angles)[:, None]
    shaped = values_in.reshape(values_in.shape[:-1] + (2, 2, pair_count))
    leading = shaped[..., 0, :]
    trailing = shaped[..., 1, :]
    turned = jnp.stack(
        [leading * cosine - trailing * sine, trailing * cosine + leading * sine], axis=-2
    )
    return turned.reshape(values_in.shape)


def per_device(tokens, query_weight, key_weight, value_weight, out_weight, query_gain, key_gain):
    query_full, key_full, value_full = (
        lax.all_gather(query_weight, "sp", axis=0, tiled=True),
        lax.all_gather(key_weight, "sp", axis=0, tiled=True),
        lax.all_gather(value_weight, "sp", axis=0, tiled=True),
    )
    query_width = query_full.shape[1]
    kv_width = key_full.shape[1]

    def project(piece, start):
        return jnp.concatenate(
            [
                jnp.dot(piece, query_full, preferred_element_type=jnp.float32).astype(jnp.bfloat16),
                jnp.dot(piece, key_full, preferred_element_type=jnp.float32).astype(jnp.bfloat16),
                jnp.dot(piece, value_full, preferred_element_type=jnp.float32).astype(jnp.bfloat16),
            ],
            axis=1,
        )

    projected = gathered_then(tokens, "tp", 0, project)
    rows = projected.shape[0]
    query_heads = query_width // HEAD_DIM
    kv_heads = kv_width // HEAD_DIM
    group_size = query_heads // kv_heads
    positions = lax.axis_index("sp") * rows + jnp.arange(rows, dtype=jnp.int32)
    queries = rotate(
        normalize(projected[:, :query_width].reshape(rows, query_heads, HEAD_DIM), query_gain),
        positions,
    ).astype(jnp.bfloat16)
    keys = rotate(
        normalize(
            projected[:, query_width : query_width + kv_width].reshape(rows, kv_heads, HEAD_DIM),
            key_gain,
        ),
        positions,
    ).astype(jnp.bfloat16)
    values = projected[:, query_width + kv_width :].reshape(rows, kv_heads, HEAD_DIM)
    grouped = queries.reshape(rows, kv_heads, group_size, HEAD_DIM)
    scale = HEAD_DIM ** (-0.5)

    def one_block(carry, block_pair):
        best, total, summed = carry
        key_block, value_block = block_pair
        scores = (
            jnp.einsum("qkgd,skd->kgqs", grouped, key_block, preferred_element_type=jnp.float32)
            * scale
        )
        fresh = jnp.maximum(best, jnp.max(scores, axis=-1))
        factor = jnp.exp(best - fresh)
        exponentials = jnp.exp(scores - fresh[..., None])
        total = total * factor + jnp.sum(exponentials, axis=-1)
        weights = exponentials.astype(jnp.bfloat16)
        summed = summed * factor[..., None] + jnp.einsum(
            "kgqs,skd->kgqd", weights, value_block, preferred_element_type=jnp.float32
        )
        return ((fresh, total, summed), None)

    def accumulate(carry, piece, start):
        key_piece, value_piece = piece
        count = key_piece.shape[0]
        block = math.gcd(count, 512)
        stacked = (
            key_piece.reshape(count // block, block, kv_heads, HEAD_DIM),
            value_piece.reshape(count // block, block, kv_heads, HEAD_DIM),
        )
        carry, _ = lax.scan(one_block, carry, stacked)
        return carry

    starting = (
        jnp.full((kv_heads, group_size, rows), -jnp.inf, jnp.float32),
        jnp.zeros((kv_heads, group_size, rows), jnp.float32),
        jnp.zeros((kv_heads, group_size, rows, HEAD_DIM), jnp.float32),
    )
    best, total, summed = over_all((keys, values), "sp", 0, accumulate, starting)
    attended = (
        jnp.transpose(summed / total[..., None], (2, 0, 1, 3))
        .reshape(rows, query_width)
        .astype(jnp.bfloat16)
    )
    out_full = lax.all_gather(out_weight, "sp", axis=1, tiled=True)

    def output_rows(start, count):
        selected = lax.dynamic_slice_in_dim(attended, start, count, 0)
        return jnp.dot(selected, out_full, preferred_element_type=jnp.float32)

    partial_value = summed_rows(output_rows, tokens.shape[0], "tp")
    scaled = partial_value * lax.rsqrt(
        jnp.mean(partial_value * partial_value, axis=-1, keepdims=True) + eps
    )
    return scaled.astype(jnp.bfloat16)


def solution(mesh):
    placed = (
        P(("sp", "tp"), None),
        P("sp", "tp"),
        P("sp", "tp"),
        P("sp", "tp"),
        P("tp", "sp"),
        P(),
        P(),
    )
    return jax.shard_map(
        per_device, mesh=mesh, in_specs=placed, out_specs=P(("sp", "tp"), None), check_vma=False
    )
```

profile of v0, /device:TPU:0, one launch (start us, length us, event | category | flops | bytes accessed | tf_op | source)
XLA Modules:
  0.0 197.9 jit_solution(10274085535248296976)
XLA Ops:
  6.5 0.0 all-gather.5.cloned.1.call-start
  6.5 0.7 all-gather.5.cloned.1.call-update
  7.3 0.0 all-gather.7.cloned.1.call-start
  7.3 0.7 all-gather.7.cloned.1.call-update
  8.0 0.0 all-gather.9.cloned.1.call-start
  8.1 0.7 all-gather.9.cloned.1.call-update
  8.7 0.0 reduce-scatter.2.cloned.1.call-start
  8.9 0.7 mul.248
  9.6 33.3 %all_gather.22 = bf16[2048,128]{1,0:T(8,128)(2,1)S(1)} all-gather(bf16[256,128]{1,0:T(8,128)(2,1)} %param.11), channel_id=1, replica_groups=mesh['sp'=8,'tp'=4] {'sp'}, dimensions={0}, use_global_device_ids=true | all-gather | bytes 589824 | tf_op jit(solution)/shard_map/all_gather | solution.py:61
  42.9 32.7 %all_gather.25 = bf16[2048,128]{1,0:T(8,128)(2,1)S(1)} all-gather(bf16[256,128]{1,0:T(8,128)(2,1)} %param.12), channel_id=1, replica_groups=mesh['sp'=8,'tp'=4] {'sp'}, dimensions={0}, use_global_device_ids=true | all-gather | bytes 589824 | tf_op jit(solution)/shard_map/all_gather | solution.py:62
  75.6 0.1 broadcast_multiply_fusion.1
  75.7 0.2 fusion.23
  75.9 0.0 all-gather.5.cloned.1.call-done
  76.0 1.8 multiply_reduce_fusion
  77.8 0.1 multiply_multiply_fusion.1
  77.9 0.3 subtract_convert_fusion.1
  78.2 0.1 copy.28
  78.3 32.7 %all_gather.23 = bf16[2048,1,128]{2,0,1:T(8,128)(2,1)S(1)} all-gather(bf16[256,1,128]{2,0,1:T(8,128)(2,1)S(1)} %copy.28), channel_id=1, replica_groups=mesh['sp'=8,'tp'=4] {'sp'}, dimensions={0}, use_global_device_ids=true | all-gather | bytes 589824 | tf_op jit(solution)/shard_map/all_gather | solution.py:22
  110.9 0.4 convolution_convert_fusion.2
  111.4 34.5 %all-gather = bf16[2048,128]{1,0:T(8,128)(2,1)} all-gather(bf16[256,128]{1,0:T(8,128)(2,1)S(1)} %convolution_convert_fusion.2), channel_id=2, replica_groups=mesh['sp'=8,'tp'=4] {'sp'}, dimensions={0}, use_global_device_ids=true | all-gather | bytes 589824 | tf_op jit(solution)/shard_map/all_gather | solution.py:22
  145.8 2.3 %fusion.31 = (f32[256,512]{1,0:T(8,128)S(1)}, f32[256,512]{1,0:T(8,128)S(1)}) fusion(bf16[256,2048]{1,0:T(8,128)(2,1)S(1)} %copy-done, bf16[2048,512]{1,0:T(8,128)(2,1)} %all-gather.7.cloned.1.call-done), kind=kOutput, calls=%fused_computation.69 | convolution fusion | flops 537264128 | bytes 4194304 | tf_op jit(solution)/shard_map/dot_general | solution.py:70
  148.1 0.2 mul.245
  148.3 0.3 reduce_sum.39
  148.7 0.1 copy.30
  148.8 0.2 copy.29
  149.0 0.1 multiply_multiply_fusion
  149.1 0.1 subtract_convert_fusion
  149.2 0.2 copy.31
  149.4 9.7 %while.15 = (s32[]{:T(128)}, f32[1,4,256]{2,1,0:T(4,128)S(1)}, f32[1,4,256]{2,1,0:T(4,128)S(1)}, f32[1,4,256,128]{3,2,1,0:T(8,128)S(1)}, bf16[4,512,1,128]{3,1,2...) while((s32[]{:T(128)}, f32[1,4,256]{2,1,0:T(4,128)S(1)}, ...), condition=%wide.region_5.6_spmd.clone, body=%wide.region_2.5_spmd.clone.sunk | while | flops 273029120 | bytes 7930477 | solution.py:123
  149.4 0.4 bitcast_reduce_fusion.2
  149.9 1.5 fusion.49
  151.4 0.4 fusion.48
  151.8 0.4 bitcast_reduce_fusion.2
  152.3 1.5 fusion.49
  153.8 0.4 fusion.48
  154.2 0.4 bitcast_reduce_fusion.2
  154.7 1.5 fusion.49
  156.2 0.4 fusion.48
  156.6 0.4 bitcast_reduce_fusion.2
  157.1 1.5 fusion.49
  158.7 0.4 fusion.48
  159.1 0.2 copy.33
  159.3 0.0 all-gather.9.cloned.1.call-done
  159.4 3.3 %convolution_convert_fusion = bf16[256,2048]{1,0:T(8,128)(2,1)} fusion(bf16[256,512]{0,1:T(8,128)(2,1)S(1)} %bitcast.98, bf16[512,2048]{1,0:T(8,128)(2,1)} %all-gather.9.cloned.1.call-done), kind=kOutput, calls=%fused_computation.25 | convolution fusion | flops 537395200 | bytes 3407872 | tf_op jit(solution)/shard_map/dot_general | solution.py:141
  162.7 0.0 reduce-scatter.2.cloned.1.call-update
  162.7 25.8 %reduce-scatter.2.cloned.1.call-done = bf16[64,2048]{1,0:T(8,128)(2,1)} async-done(((bf16[256,2048]{1,0:T(8,128)(2,1)}), bf16[64,2048]{1,0:T(8,128)(2,1)}) %reduce-scatter.2.cloned.1.call-update) | async-done | bytes 262160 | tf_op jit(solution)/shard_map/reduce_scatter | solution.py:28
  188.5 1.1 fusion.20
  189.6 1.8 fusion.21
  (28 shorter events, 0.3 us)
Async XLA Ops:
  6.5 71.3 %copy-start.1 = (f32[128]{0:T(128)S(1)}, f32[128]{0:T(128)}, u32[]{:S(2)}) copy-start(f32[128]{0:T(128)} %param.15) | copy-start | bytes 1540
  6.5 69.4 %all-gather.5.cloned.1.call-start = ((), (), s32[]{:S(2)}) async-start(), calls=%async_computation.1 | async-start | bytes 1310720 | tf_op jit(solution)/shard_map/all_gather | solution.py:17
  7.3 138.6 %all-gather.7.cloned.1.call-start = ((), (), s32[]{:S(2)}) async-start(), calls=%async_computation.2 | async-start | bytes 2359296 | tf_op jit(solution)/shard_map/all_gather | solution.py:60
  8.0 151.3 %all-gather.9.cloned.1.call-start = ((), (), s32[]{:S(2)}) async-start(), calls=%async_computation.3 | async-start | bytes 2359296 | tf_op jit(solution)/shard_map/all_gather | solution.py:137
  8.7 179.8 %reduce-scatter.2.cloned.1.call-start = ((), (), s32[]{:S(2)}) async-start(), calls=%async_computation.4 | async-start | bytes 1310720 | tf_op jit(solution)/shard_map/reduce_scatter | solution.py:28
  75.9 35.0 %copy-start = (bf16[256,2048]{1,0:T(8,128)(2,1)S(1)}, bf16[256,2048]{1,0:T(8,128)(2,1)}, u32[]{:S(2)}) copy-start(bf16[256,2048]{1,0:T(8,128)(2,1)} %all-gather.5.cloned.1.call-done) | copy-start | bytes 3145732
Sparse Core Ops, SparseCore 0:
  8.9 19.3 all-gather.4
  30.4 55.3 all-gather.6
  87.8 55.2 all-gather.8
  162.8 25.6 reduce-scatter.1
where the time goes:
time: 198 us
  blocking collectives  133 us (67%)
  waiting for transfers between devices  28 us (14%)
  matrix products  15.8 us (8%)
  between operations  13.3 us (7%)
  other arithmetic  5.75 us (3%)
    all_gather x2, blocking collectives, over_all(): lax.all_gather(a, axis, axis=dim, tiled=True)  67.1 us
    all_gather x1, blocking collectives, per_device(): lax.all_gather(key_weight, 'sp', axis=0, tiled=True)  33.3 us
    all_gather x1, blocking collectives, per_device(): lax.all_gather(value_weight, 'sp', axis=0, tiled=True)  32.7 us
    reduce_scatter x1, waiting for transfers between devices, summed_rows(): lax.psum_scatter(everything.astype(jnp.bfloat16), axis, scatter_dimension...  25.8 us
    dot_general x4, matrix products, one_block(): jnp.einsum('kgqs,skd->kgqd', weights, value_block, preferred_element_type...  6.14 us
  transfers between devices with their start and end apart: 4, of which 1 were waited for; matrix products, arithmetic and copies ran while one was open for 9% of the time, Pallas kernels for 0%

commit v1 on v0

v1 whole, which is shorter than its diff:
```python
import functools
import math

import jax
import jax.numpy as jnp
from jax import lax
from jax.experimental import pallas as pl
from jax.experimental.pallas import tpu as pltpu
from jax.sharding import PartitionSpec as P

HEAD_DIM = 128
GRID_W = 64
MESH = pl.DeviceIdType.MESH

eps = 1e-06
rope_base = 10000.0
BLOCK = 256
NT = (((1,), (1,)), ((), ()))


def remote(src, dst, send_sem, recv_sem, device):
    return pltpu.make_async_remote_copy(
        src_ref=src,
        dst_ref=dst,
        send_sem=send_sem,
        recv_sem=recv_sem,
        device_id=device,
        device_id_type=MESH,
    )


class Line:
    def __init__(self, own, buffer, size, send, recv, s, t, lines):
        self.own, self.buffer, self.size = own, buffer, size
        self.send, self.recv, self.s, self.t, self.lines = send, recv, s, t, lines
        self.line, self.half = s // 2, lax.rem(s, 2)

    def place(self, source):
        return self.buffer.at[pl.ds(pl.multiple_of(source * self.size, self.size), self.size)]

    def along(self, source, way, src=None):
        where = self.place(source)
        return remote(
            where if src is None else src,
            where,
            self.send.at[way, source],
            self.recv.at[source],
            (self.s + (2 if way else -2), self.t),
        )

    def push(self, source, way, src=None):
        @pl.when(self.line < self.lines - 1 if way else self.line > 0)
        def _():
            self.along(source, way, src).start()

    def pair(self):
        return remote(
            self.own.at[1 - self.half],
            self.place(self.s),
            self.send.at[2, self.s],
            self.recv.at[self.s],
            (self.s + 1 - 2 * self.half, self.t),
        )

    def local(self):
        return pltpu.make_async_copy(
            self.own.at[self.half], self.place(self.s), self.send.at[2, self.s + 1 - 2 * self.half]
        )

    def push_own(self):
        self.push(self.s, 0, self.own.at[self.half])
        self.push(self.s, 1, self.own.at[self.half])

    def arrived(self, source):
        self.along(source, 0).wait_recv()

    def push_pair(self):
        other = self.s + 1 - 2 * self.half
        self.arrived(other)
        self.push(other, 0)
        self.push(other, 1)

    def step(self, distance):
        for j in range(2):
            @pl.when(self.line >= distance)
            def _():
                source = 2 * (self.line - distance) + j
                self.arrived(source)
                self.push(source, 1)

            @pl.when(self.line + distance < self.lines)
            def _():
                source = 2 * (self.line + distance) + j
                self.arrived(source)
                self.push(source, 0)

    def finish(self):
        self.pair().wait_send()

        def one(source, _):
            @pl.when((source // 2 <= self.line) & (self.line < self.lines - 1))
            def _():
                self.along(source, 1).wait_send()

            @pl.when((source // 2 >= self.line) & (self.line > 0))
            def _():
                self.along(source, 0).wait_send()

            return 0

        lax.fori_loop(0, 2 * self.lines, one, 0)


def kernel(
    S, T,
    x_ref, w_ref, o_ref, qg_ref, kg_ref, out_ref,
    X, W, OW, KV, Q, A, C, SN, best, total, summed, PS, SB, RC, SF, RF,
    xs_sem, xr_sem, ws_sem, wr_sem, os_sem, or_sem, ks_sem, kr_sem, kp_sem, kq_sem,
    cs_sem, fs_sem, fr_sem,
):
    L, N = S // 2, 2 * T
    R, D = x_ref.shape
    M = N * R
    wr, wc = w_ref.shape[1:]
    oc, hw = o_ref.shape[1:]
    heads = hw // HEAD_DIM
    s, t = lax.axis_index("sp"), lax.axis_index("tp")
    line, half = s // 2, lax.rem(s, 2)
    core, across = lax.rem(t, 2), t // 2
    mate = t + 1 - 2 * core
    other = s + 1 - 2 * half
    H = T // 2
    slot = half * T + t
    h = half * H + across

    def plane(b):
        return (2 * line + b // T, lax.rem(b, T))

    barrier = pltpu.get_barrier_semaphore()
    for i in range(1, N):
        pl.semaphore_signal(
            barrier, inc=1, device_id=plane(lax.rem(slot + i, N)), device_id_type=MESH
        )

    @pl.when(line > 0)
    def _():
        pl.semaphore_signal(barrier, inc=1, device_id=(s - 2, t), device_id_type=MESH)

    @pl.when(line < L - 1)
    def _():
        pl.semaphore_signal(barrier, inc=1, device_id=(s + 2, t), device_id_type=MESH)

    pl.semaphore_wait(
        barrier,
        N - 1 + jnp.where(line > 0, 1, 0) + jnp.where(line < L - 1, 1, 0),
    )

    weights = Line(w_ref, W, wr, ws_sem, wr_sem, s, t, L)
    outs = Line(o_ref, OW, oc, os_sem, or_sem, s, t, L)

    def rows(b):
        return X.at[pl.ds(pl.multiple_of(b * R, R), R)]

    def peer(hh):
        return hh // H, 2 * lax.rem(hh, H) + core

    def token_send(i):
        ph, pt = peer(lax.rem(h + i, T))
        return remote(x_ref, rows(slot), xs_sem.at[i], xr_sem.at[slot], (2 * line + ph, pt))

    def token_block(i):
        ph, pt = peer(lax.rem(h + T - i, T))
        return ph * T + pt

    def token_mate(i):
        b = token_block(i)
        return remote(
            x_ref if i == 0 else rows(b), rows(b), xs_sem.at[T + i], xr_sem.at[b], (s, mate)
        )

    weights.pair().start()
    weights.push_own()
    for i in range(1, T):
        token_send(i).start()
    token_mate(0).start()
    outs.pair().start()
    weights.local().start()
    outs.local().start()
    own_tokens = pltpu.make_async_copy(x_ref, rows(slot), xs_sem.at[0])
    own_tokens.start()

    lane = lax.broadcasted_iota(jnp.int32, (BLOCK, HEAD_DIM), 1)
    pairs = HEAD_DIM // 4
    rate = jnp.exp(
        lax.rem(lane, pairs).astype(jnp.float32) * (-math.log(rope_base) / pairs)
    )
    by_row = lane < 2 * pairs
    leading = lax.rem(lane, 2 * pairs) < pairs
    for rb in range(M // BLOCK):
        position = (
            line * M + rb * BLOCK + lax.broadcasted_iota(jnp.int32, (BLOCK, HEAD_DIM), 0)
        )
        grid = jnp.where(by_row, position // GRID_W, lax.rem(position, GRID_W))
        angle = grid.astype(jnp.float32) * rate
        C[pl.ds(rb * BLOCK, BLOCK), :] = jnp.cos(angle)
        sine = jnp.sin(angle)
        SN[pl.ds(rb * BLOCK, BLOCK), :] = jnp.where(leading, -sine, sine)
    best[...] = jnp.full_like(best, -jnp.inf)
    total[...] = jnp.zeros_like(total)
    summed[...] = jnp.zeros_like(summed)

    weights.push_pair()
    weights.step(1)
    for i in range(1, T):
        remote(x_ref, rows(token_block(i)), xs_sem.at[i], xr_sem.at[token_block(i)], (s, mate)).wait_recv()
        token_mate(i).start()

    def weight_step(d, _):
        weights.step(d)
        return 0

    lax.fori_loop(2, L, weight_step, 0)
    outs.push_own()
    outs.push_pair()
    own_tokens.wait()
    weights.local().wait()
    outs.local().wait()

    def mate_block(i):
        hh = lax.rem(h + T - i, T)
        return (hh // H) * T + 2 * lax.rem(hh, H) + 1 - core

    for i in range(T):
        b = mate_block(i)
        remote(x_ref, rows(b), xs_sem.at[i], xr_sem.at[b], (s, mate)).wait_recv()

    def turned(raw, gain, at):
        n = raw * lax.rsqrt(jnp.mean(raw * raw, axis=-1, keepdims=True) + eps) * gain
        partner = jnp.where(
            leading, pltpu.roll(n, HEAD_DIM - pairs, 1), pltpu.roll(n, pairs, 1)
        )
        return (n * C[at, :] + partner * SN[at, :]).astype(jnp.bfloat16)

    for rb in range(M // BLOCK):
        at = pl.ds(rb * BLOCK, BLOCK)
        raw = jnp.dot(X[at, :], W[...], preferred_element_type=jnp.float32).astype(jnp.bfloat16)
        mine = pl.ds(pl.multiple_of(line * M + rb * BLOCK, BLOCK), BLOCK)
        kv = raw[:, hw:]

        @pl.when(half == 0)
        def _():
            KV[0, mine, :] = turned(kv.astype(jnp.float32), kg_ref[...], at)

        @pl.when(half == 1)
        def _():
            KV[1, mine, :] = kv

        for j in range(heads):
            part = raw[:, j * HEAD_DIM : (j + 1) * HEAD_DIM].astype(jnp.float32)
            Q[pl.ds(j * M + rb * BLOCK, BLOCK), :] = turned(part, qg_ref[...], at)

    def chunk(which, source):
        return KV.at[which, pl.ds(pl.multiple_of(source * M, M), M)]

    def kv_along(source, way):
        return remote(
            chunk(half, source), chunk(half, source), ks_sem.at[way, source], kr_sem.at[source],
            (s + (2 if way else -2), t),
        )

    def kv_pair(source, which):
        return remote(
            chunk(which, source), chunk(which, source), kp_sem.at[source], kq_sem.at[source],
            (other, t),
        )

    def kv_push(source, way):
        @pl.when(line < L - 1 if way else line > 0)
        def _():
            kv_along(source, way).start()

    def kv_step(d):
        for way in (1, 0):
            source = line - d if way else line + d

            @pl.when(line >= d if way else line + d < L)
            def _():
                kv_along(source, way).wait_recv()
                kv_push(source, way)
                kv_pair(source, half).start()

    factor = HEAD_DIM ** (-0.5) * math.log2(math.e)

    def attend(source):
        kv_pair(source, 1 - half).wait_recv()
        at = pl.ds(pl.multiple_of(source * M, M), M)

        def one(r, _):
            q_at = pl.ds(pl.multiple_of(r * BLOCK, BLOCK), BLOCK)
            scores = (
                lax.dot_general(Q[q_at, :], KV[0, at, :], NT, preferred_element_type=jnp.float32)
                * factor
            )
            old = best[q_at, :]
            fresh = jnp.maximum(old, jnp.max(scores, axis=-1, keepdims=True))
            shrink = jnp.exp2(old - fresh)
            exponentials = jnp.exp2(scores - fresh)
            best[q_at, :] = fresh
            total[q_at, :] = total[q_at, :] * shrink + jnp.sum(exponentials, axis=-1, keepdims=True)
            summed[q_at, :] = summed[q_at, :] * shrink + jnp.dot(
                exponentials.astype(jnp.bfloat16), KV[1, at, :], preferred_element_type=jnp.float32
            )
            return 0

        lax.fori_loop(0, heads * M // BLOCK, one, 0)

    def attend_at(d):
        @pl.when(line >= d)
        def _():
            attend(line - d)

        @pl.when(line + d < L)
        def _():
            attend(line + d)

    kv_push(line, 0)
    kv_push(line, 1)
    kv_pair(line, half).start()
    kv_step(1)
    attend(line)

    def kv_round(d, _):
        kv_step(d)
        attend_at(d - 1)
        return 0

    lax.fori_loop(2, L, kv_round, 0)
    outs.step(1)
    attend_at(L - 1)

    def out_round(d, _):
        outs.step(d)
        return 0

    lax.fori_loop(2, L, out_round, 0)

    for ph in range(2):
        for pt in range(T):
            source = (ph * T + pt) * R
            target = (pt % 2) * T * R + (ph * H + pt // 2) * R
            for j in range(heads):
                at = pl.ds(j * M + source, R)
                A[pl.ds(target, R), j * HEAD_DIM : (j + 1) * HEAD_DIM] = (
                    summed[at, :] / total[at, :]
                ).astype(jnp.bfloat16)

    TR = T * R
    width = min(D, 512)

    def product(parity, cb):
        return lax.dot_general(
            A[pl.ds(pl.multiple_of(parity * TR, TR), TR), :],
            OW[pl.ds(cb * width, width), :],
            NT,
            preferred_element_type=jnp.float32,
        )

    to_mate = remote(SB, RC, cs_sem.at[0], cs_sem.at[1], (s, mate))
    for cb in range(D // width):
        SB[:, cb * width : (cb + 1) * width] = product(1 - core, cb).astype(jnp.bfloat16)
    to_mate.start()
    for cb in range(D // width):
        PS[:, cb * width : (cb + 1) * width] = product(core, cb)
    to_mate.wait_recv()

    def final_send(i):
        ph, pt = peer(lax.rem(h + i, T))
        return remote(
            SF.at[i - 1], RF.at[i - 1], fs_sem.at[i - 1], fr_sem.at[i - 1], (2 * line + ph, pt)
        )

    def reduced(hh):
        at = pl.ds(pl.multiple_of(hh * R, R), R)
        return PS[at, :] + RC[at, :].astype(jnp.float32)

    for i in range(1, T):
        SF[i - 1] = reduced(lax.rem(h + i, T)).astype(jnp.bfloat16)
        final_send(i).start()
    result = reduced(h)
    for i in range(1, T):
        final_send(i).wait_recv()
        result = result + RF[i - 1].astype(jnp.float32)
    out_ref[...] = (
        result * lax.rsqrt(jnp.mean(result * result, axis=-1, keepdims=True) + eps)
    ).astype(out_ref.dtype)

    weights.finish()
    outs.finish()
    for i in range(1, T):
        token_send(i).wait_send()
        final_send(i).wait_send()
    for i in range(T):
        token_mate(i).wait_send()
    to_mate.wait_send()

    def kv_done(source, _):
        kv_pair(source, half).wait_send()

        @pl.when((source <= line) & (line < L - 1))
        def _():
            kv_along(source, 1).wait_send()

        @pl.when((source >= line) & (line > 0))
        def _():
            kv_along(source, 0).wait_send()

        return 0

    lax.fori_loop(0, L, kv_done, 0)


def per_device(tokens, query_weight, key_weight, value_weight, out_weight, query_gain, key_gain):
    S, T = lax.axis_size("sp"), lax.axis_size("tp")
    L = S // 2
    R, D = tokens.shape
    M = 2 * T * R
    hw = query_weight.shape[1] // 2
    heads = hw // HEAD_DIM
    wr, oc = query_weight.shape[0], out_weight.shape[1]
    wc = hw + HEAD_DIM
    w = jnp.stack(
        [
            jnp.concatenate([query_weight[:, :hw], key_weight], axis=1),
            jnp.concatenate([query_weight[:, hw:], value_weight], axis=1),
        ]
    )
    o = jnp.swapaxes(out_weight.reshape(2, hw, oc), 1, 2)
    vmem = pl.BlockSpec(memory_space=pltpu.VMEM)
    bf, f32 = jnp.bfloat16, jnp.float32
    dma = pltpu.SemaphoreType.DMA
    return pl.pallas_call(
        functools.partial(kernel, S, T),
        out_shape=jax.ShapeDtypeStruct((R, D), bf),
        in_specs=[vmem] * 5,
        out_specs=vmem,
        scratch_shapes=[
            pltpu.VMEM((M, D), bf),
            pltpu.VMEM((S * wr, wc), bf),
            pltpu.VMEM((S * oc, hw), bf),
            pltpu.VMEM((2, L * M, HEAD_DIM), bf),
            pltpu.VMEM((heads * M, HEAD_DIM), bf),
            pltpu.VMEM((M, hw), bf),
            pltpu.VMEM((M, HEAD_DIM), f32),
            pltpu.VMEM((M, HEAD_DIM), f32),
            pltpu.VMEM((heads * M, 1), f32),
            pltpu.VMEM((heads * M, 1), f32),
            pltpu.VMEM((heads * M, HEAD_DIM), f32),
            pltpu.VMEM((T * R, D), f32),
            pltpu.VMEM((T * R, D), bf),
            pltpu.VMEM((T * R, D), bf),
            pltpu.VMEM((T - 1, R, D), bf),
            pltpu.VMEM((T - 1, R, D), bf),
            dma((2 * T,)),
            dma((2 * T,)),
            dma((3, S)),
            dma((S,)),
            dma((3, S)),
            dma((S,)),
            dma((2, L)),
            dma((L,)),
            dma((L,)),
            dma((L,)),
            dma((2,)),
            dma((T - 1,)),
            dma((T - 1,)),
        ],
        compiler_params=pltpu.CompilerParams(collective_id=0, has_side_effects=True),
    )(tokens, w, o, query_gain.reshape(1, HEAD_DIM), key_gain.reshape(1, HEAD_DIM))


def solution(mesh):
    placed = (
        P(("sp", "tp"), None),
        P("sp", "tp"),
        P("sp", "tp"),
        P("sp", "tp"),
        P("tp", "sp"),
        P(),
        P(),
    )
    return jax.shard_map(
        per_device, mesh=mesh, in_specs=placed, out_specs=P(("sp", "tp"), None), check_vma=False
    )
```

time: 198 us -> 85.2 us (0.43)
  blocking collectives: 133 us -> 0 us
  Pallas kernels: 0 us -> 80.2 us
  waiting for transfers between devices: 28 us -> 0 us
  matrix products: 15.8 us -> 0 us
  between operations: 13.3 us -> 0.05 us
  other arithmetic: 5.75 us -> 0.84 us
  local copies, waits for them, and re-layouts: 1.7 us -> 3.69 us
    all_gather x4 -> x0, blocking collectives: 133 us -> none  [the longest x2 67.1 us: over_all(): lax.all_gather(a, axis, axis=dim, tiled=True)]
    pallas_call x0 -> x1, Pallas kernels: none -> 80.2 us  [per_device(): pl.pallas_call(functools.partial(kernel, S, T), out_shape=jax.ShapeDtypeS...]
    reduce_scatter x1 -> x0, waiting for transfers between devices: 25.8 us -> none  [summed_rows(): lax.psum_scatter(everything.astype(jnp.bfloat16), axis, scatter_dimension...]
    dot_general x12 -> x0, matrix products: 15.8 us -> none  [the longest x4 6.14 us: one_block(): jnp.einsum('kgqs,skd->kgqd', weights, value_block, preferred_element_type...]
    reduce_sum x6 -> x0, other arithmetic: 2.9 us -> none  [the longest x4 1.45 us: one_block(): total = total * factor + jnp.sum(exponentials, axis=-1)]
    unnamed x4 -> x0, waiting for transfers between devices: 2.1 us -> none
  transfers between devices with their start and end apart: 4 -> 0, of which waited for: 1 -> 0; matrix products, arithmetic and copies ran while one was open for 9% -> 0% of each run, Pallas kernels for 0% -> 0%
where the time goes in v1:
time: 85.2 us; the launch traced here: 84.8 us
  Pallas kernels  80.2 us (94%)
  local copies, waits for them, and re-layouts  3.69 us (4%)
    pallas_call x1, Pallas kernels, per_device(): pl.pallas_call(functools.partial(kernel, S, T), out_shape=jax.ShapeDtypeS...  80.2 us
    unnamed x7, local copies, waits for them, and re-layouts  1.83 us

profile of v1, /device:TPU:0, one launch (start us, length us, event | category | flops | bytes accessed | tf_op | source)
XLA Modules:
  0.0 84.8 jit_solution(11638847092638777360)
XLA Ops:
  0.0 0.0 copy-start.2
  0.0 0.0 copy-start.1
  0.0 1.0 %fusion = (bf16[256,256]{1,0:T(8,128)(2,1)S(1)}, bf16[256,256]{1,0:T(8,128)(2,1)S(1)}) fusion(bf16[256,512]{1,0:T(8,128)(2,1)} %param.8), kind=kLoop, calls=%fused_computation.3 | loop fusion | bytes 524288 | tf_op jit(solution)/shard_map/slice | solution.py:433
  1.0 0.0 copy-done.2
  1.0 0.0 copy-done.1
  1.1 0.0 copy-start
  1.1 0.8 pad_maximum_fusion.w_ref
  1.9 0.1 copy-done
  2.1 0.8 copy.8
  2.9 80.2 %shard_map.73 = bf16[64,2048]{1,0:T(8,128)(2,1)} custom-call(bf16[64,2048]{1,0:T(8,128)(2,1)} %x_ref.1, bf16[2,256,384]{2,1,0:T(8,128)(2,1)} %pad_maximum_fusion.w_ref, bf16[2,256,256]{2,1,0:T(8,128)(2,1)} %bitcast.8, f32[1,128]{1,0:T(1,128)} %bitcast.10, f32[1,128]{1,0:T(1,128)} %bitcast.11), custom_call_target="tpu_custom_call" | custom-call | tf_op jit(solution)/shard_map/pallas_call | solution.py:441
  83.1 1.7 %copy.10 = bf16[64,2048]{1,0:T(8,128)(2,1)} copy(bf16[64,2048]{1,0:T(8,128)(2,1)} %shard_map.73) | data formatting | bytes 524288
  (1 shorter events, 0.0 us)
Async XLA Ops:
  0.0 1.0 %copy-start.2 = (bf16[256,128]{1,0:T(8,128)(2,1)S(1)}, bf16[256,128]{1,0:T(8,128)(2,1)}, u32[]{:S(2)}) copy-start(bf16[256,128]{1,0:T(8,128)(2,1)} %param.10) | copy-start | bytes 196612
  0.0 1.0 %copy-start.1 = (bf16[256,128]{1,0:T(8,128)(2,1)S(1)}, bf16[256,128]{1,0:T(8,128)(2,1)}, u32[]{:S(2)}) copy-start(bf16[256,128]{1,0:T(8,128)(2,1)} %param.9) | copy-start | bytes 196612
  1.1 1.0 %copy-start = (bf16[512,256]{1,0:T(8,128)(2,1)S(1)}, bf16[512,256]{1,0:T(8,128)(2,1)}, u32[]{:S(2)}) copy-start(bf16[512,256]{1,0:T(8,128)(2,1)} %param.11) | copy-start | bytes 786436

commit v2 on v1

--- a/solution.py
+++ b/solution.py
@@ -113,15 +113,15 @@
 
 def kernel(
     S, T,
-    x_ref, w_ref, o_ref, qg_ref, kg_ref, out_ref,
-    X, W, OW, KV, Q, A, C, SN, best, total, summed, PS, SB, RC, SF, RF,
-    xs_sem, xr_sem, ws_sem, wr_sem, os_sem, or_sem, ks_sem, kr_sem, kp_sem, kq_sem,
-    cs_sem, fs_sem, fr_sem,
+    x_ref, w_ref, v_ref, o_ref, qg_ref, kg_ref, out_ref,
+    X, W, WV, OW, KV, Q, A, C, SN, best, total, summed, PS, SB, RC, SF, RF,
+    xs_sem, xr_sem, ws_sem, wr_sem, vs_sem, vr_sem, os_sem, or_sem, ks_sem, kr_sem, kp_sem, kq_sem,
+    cs_sem, cr_sem, fs_sem, fr_sem,
 ):
     L, N = S // 2, 2 * T
     R, D = x_ref.shape
     M = N * R
-    wr, wc = w_ref.shape[1:]
+    wr = w_ref.shape[1]
     oc, hw = o_ref.shape[1:]
     heads = hw // HEAD_DIM
     s, t = lax.axis_index("sp"), lax.axis_index("tp")
@@ -156,6 +156,7 @@
     )
 
     weights = Line(w_ref, W, wr, ws_sem, wr_sem, s, t, L)
+    kv_weights = Line(v_ref, WV, wr, vs_sem, vr_sem, s, t, L)
     outs = Line(o_ref, OW, oc, os_sem, or_sem, s, t, L)
 
     def rows(b):
@@ -178,12 +179,14 @@
             x_ref if i == 0 else rows(b), rows(b), xs_sem.at[T + i], xr_sem.at[b], (s, mate)
         )
 
+    kv_weights.pair().start()
+    kv_weights.push_own()
     weights.pair().start()
-    weights.push_own()
     for i in range(1, T):
         token_send(i).start()
     token_mate(0).start()
     outs.pair().start()
+    kv_weights.local().start()
     weights.local().start()
     outs.local().start()
     own_tokens = pltpu.make_async_copy(x_ref, rows(slot), xs_sem.at[0])
@@ -209,22 +212,23 @@
     total[...] = jnp.zeros_like(total)
     summed[...] = jnp.zeros_like(summed)
 
+    kv_weights.push_pair()
+
+    def kv_weight_step(d, _):
+        kv_weights.step(d)
+        return 0
+
+    lax.fori_loop(1, L - 1, kv_weight_step, 0)
+    weights.push_own()
     weights.push_pair()
-    weights.step(1)
+    kv_weights.step(L - 1)
     for i in range(1, T):
         remote(x_ref, rows(token_block(i)), xs_sem.at[i], xr_sem.at[token_block(i)], (s, mate)).wait_recv()
         token_mate(i).start()
 
-    def weight_step(d, _):
-        weights.step(d)
-        return 0
-
-    lax.fori_loop(2, L, weight_step, 0)
-    outs.push_own()
-    outs.push_pair()
+    weights.step(1)
     own_tokens.wait()
-    weights.local().wait()
-    outs.local().wait()
+    kv_weights.local().wait()
 
     def mate_block(i):
         hh = lax.rem(h + T - i, T)
@@ -243,9 +247,8 @@
 
     for rb in range(M // BLOCK):
         at = pl.ds(rb * BLOCK, BLOCK)
-        raw = jnp.dot(X[at, :], W[...], preferred_element_type=jnp.float32).astype(jnp.bfloat16)
+        kv = jnp.dot(X[at, :], WV[...], preferred_element_type=jnp.float32).astype(jnp.bfloat16)
         mine = pl.ds(pl.multiple_of(line * M + rb * BLOCK, BLOCK), BLOCK)
-        kv = raw[:, hw:]
 
         @pl.when(half == 0)
         def _():
@@ -254,10 +257,6 @@
         @pl.when(half == 1)
         def _():
             KV[1, mine, :] = kv
-
-        for j in range(heads):
-            part = raw[:, j * HEAD_DIM : (j + 1) * HEAD_DIM].astype(jnp.float32)
-            Q[pl.ds(j * M + rb * BLOCK, BLOCK), :] = turned(part, qg_ref[...], at)
 
     def chunk(which, source):
         return KV.at[which, pl.ds(pl.multiple_of(source * M, M), M)]
@@ -326,23 +325,33 @@
     kv_push(line, 0)
     kv_push(line, 1)
     kv_pair(line, half).start()
-    kv_step(1)
+
+    def weight_step(d, _):
+        kv_step(d - 1)
+        weights.step(d)
+        return 0
+
+    lax.fori_loop(2, L, weight_step, 0)
+    kv_step(L - 1)
+    outs.push_own()
+    outs.push_pair()
+    weights.local().wait()
+    outs.local().wait()
+    for rb in range(M // BLOCK):
+        at = pl.ds(rb * BLOCK, BLOCK)
+        raw = jnp.dot(X[at, :], W[...], preferred_element_type=jnp.float32).astype(jnp.bfloat16)
+        for j in range(heads):
+            part = raw[:, j * HEAD_DIM : (j + 1) * HEAD_DIM].astype(jnp.float32)
+            Q[pl.ds(j * M + rb * BLOCK, BLOCK), :] = turned(part, qg_ref[...], at)
+
     attend(line)
-
-    def kv_round(d, _):
-        kv_step(d)
-        attend_at(d - 1)
+    outs.step(1)
+
+    def attend_round(d, _):
+        attend_at(d)
         return 0
 
-    lax.fori_loop(2, L, kv_round, 0)
-    outs.step(1)
-    attend_at(L - 1)
-
-    def out_round(d, _):
-        outs.step(d)
-        return 0
-
-    lax.fori_loop(2, L, out_round, 0)
+    lax.fori_loop(1, L, attend_round, 0)
 
     for ph in range(2):
         for pt in range(T):
@@ -355,53 +364,93 @@
                 ).astype(jnp.bfloat16)
 
     TR = T * R
-    width = min(D, 512)
-
-    def product(parity, cb):
+    width = 2 * oc
+
+    def product(parity, g):
         return lax.dot_general(
             A[pl.ds(pl.multiple_of(parity * TR, TR), TR), :],
-            OW[pl.ds(cb * width, width), :],
+            OW[pl.ds(pl.multiple_of(g * width, width), width), :],
             NT,
             preferred_element_type=jnp.float32,
         )
 
-    to_mate = remote(SB, RC, cs_sem.at[0], cs_sem.at[1], (s, mate))
-    for cb in range(D // width):
-        SB[:, cb * width : (cb + 1) * width] = product(1 - core, cb).astype(jnp.bfloat16)
-    to_mate.start()
-    for cb in range(D // width):
-        PS[:, cb * width : (cb + 1) * width] = product(core, cb)
-    to_mate.wait_recv()
-
-    def final_send(i):
+    def to_mate(g):
+        return remote(SB.at[g], RC.at[g], cs_sem.at[g], cr_sem.at[g], (s, mate))
+
+    def final_send(g, i):
         ph, pt = peer(lax.rem(h + i, T))
         return remote(
-            SF.at[i - 1], RF.at[i - 1], fs_sem.at[i - 1], fr_sem.at[i - 1], (2 * line + ph, pt)
-        )
-
-    def reduced(hh):
+            SF.at[g, i - 1], RF.at[g, i - 1], fs_sem.at[g, i - 1], fr_sem.at[g, i - 1],
+            (2 * line + ph, pt),
+        )
+
+    def reduced(g, hh):
         at = pl.ds(pl.multiple_of(hh * R, R), R)
-        return PS[at, :] + RC[at, :].astype(jnp.float32)
-
-    for i in range(1, T):
-        SF[i - 1] = reduced(lax.rem(h + i, T)).astype(jnp.bfloat16)
-        final_send(i).start()
-    result = reduced(h)
-    for i in range(1, T):
-        final_send(i).wait_recv()
-        result = result + RF[i - 1].astype(jnp.float32)
-    out_ref[...] = (
-        result * lax.rsqrt(jnp.mean(result * result, axis=-1, keepdims=True) + eps)
-    ).astype(out_ref.dtype)
-
+        return PS[g, at, :] + RC[g, at, :].astype(jnp.float32)
+
+    def multiply(g):
+        SB[g] = product(1 - core, g).astype(jnp.bfloat16)
+        to_mate(g).start()
+        PS[g] = product(core, g)
+
+    def spread(g):
+        to_mate(g).wait_recv()
+        for i in range(1, T):
+            SF[g, i - 1] = reduced(g, lax.rem(h + i, T)).astype(jnp.bfloat16)
+            final_send(g, i).start()
+
+    def both_ways(act, d):
+        @pl.when(line >= d)
+        def _():
+            act(line - d)
+
+        @pl.when(line + d < L)
+        def _():
+            act(line + d)
+
+    multiply(line)
+    both_ways(multiply, 1)
+    spread(line)
+
+    def out_round(d, _):
+        both_ways(spread, d - 1)
+        outs.step(d)
+        both_ways(multiply, d)
+        return 0
+
+    lax.fori_loop(2, L, out_round, 0)
+    both_ways(spread, L - 1)
+
+    def gather_group(g, squares):
+        result = reduced(g, h)
+        for i in range(1, T):
+            final_send(g, i).wait_recv()
+            result = result + RF[g, i - 1].astype(jnp.float32)
+        PS[g, pl.ds(pl.multiple_of(h * R, R), R), :] = result
+        return squares + jnp.sum(result * result, axis=-1, keepdims=True)
+
+    squares = lax.fori_loop(0, L, gather_group, jnp.zeros((R, 1), jnp.float32))
+    norm = lax.rsqrt(squares / D + eps)
+    for g in range(L):
+        out_ref[:, g * width : (g + 1) * width] = (
+            PS[g, pl.ds(pl.multiple_of(h * R, R), R), :] * norm
+        ).astype(out_ref.dtype)
+
+    kv_weights.finish()
     weights.finish()
     outs.finish()
     for i in range(1, T):
         token_send(i).wait_send()
-        final_send(i).wait_send()
     for i in range(T):
         token_mate(i).wait_send()
-    to_mate.wait_send()
+
+    def group_done(g, _):
+        to_mate(g).wait_send()
+        for i in range(1, T):
+            final_send(g, i).wait_send()
+        return 0
+
+    lax.fori_loop(0, L, group_done, 0)
 
     def kv_done(source, _):
         kv_pair(source, half).wait_send()
@@ -427,13 +476,8 @@
     hw = query_weight.shape[1] // 2
     heads = hw // HEAD_DIM
     wr, oc = query_weight.shape[0], out_weight.shape[1]
-    wc = hw + HEAD_DIM
-    w = jnp.stack(
-        [
-            jnp.concatenate([query_weight[:, :hw], key_weight], axis=1),
-            jnp.concatenate([query_weight[:, hw:], value_weight], axis=1),
-        ]
-    )
+    w = jnp.stack([query_weight[:, :hw], query_weight[:, hw:]])
+    v = jnp.stack([key_weight, value_weight])
     o = jnp.swapaxes(out_weight.reshape(2, hw, oc), 1, 2)
     vmem = pl.BlockSpec(memory_space=pltpu.VMEM)
     bf, f32 = jnp.bfloat16, jnp.float32
@@ -441,11 +485,12 @@
     return pl.pallas_call(
         functools.partial(kernel, S, T),
         out_shape=jax.ShapeDtypeStruct((R, D), bf),
-        in_specs=[vmem] * 5,
+        in_specs=[vmem] * 6,
         out_specs=vmem,
         scratch_shapes=[
             pltpu.VMEM((M, D), bf),
-            pltpu.VMEM((S * wr, wc), bf),
+            pltpu.VMEM((S * wr, hw), bf),
+            pltpu.VMEM((S * wr, HEAD_DIM), bf),
             pltpu.VMEM((S * oc, hw), bf),
             pltpu.VMEM((2, L * M, HEAD_DIM), bf),
             pltpu.VMEM((heads * M, HEAD_DIM), bf),
@@ -455,13 +500,15 @@
             pltpu.VMEM((heads * M, 1), f32),
             pltpu.VMEM((heads * M, 1), f32),
             pltpu.VMEM((heads * M, HEAD_DIM), f32),
-            pltpu.VMEM((T * R, D), f32),
-            pltpu.VMEM((T * R, D), bf),
-            pltpu.VMEM((T * R, D), bf),
-            pltpu.VMEM((T - 1, R, D), bf),
-            pltpu.VMEM((T - 1, R, D), bf),
+            pltpu.VMEM((L, T * R, 2 * oc), f32),
+            pltpu.VMEM((L, T * R, 2 * oc), bf),
+            pltpu.VMEM((L, T * R, 2 * oc), bf),
+            pltpu.VMEM((L, T - 1, R, 2 * oc), bf),
+            pltpu.VMEM((L, T - 1, R, 2 * oc), bf),
             dma((2 * T,)),
             dma((2 * T,)),
+            dma((3, S)),
+            dma((S,)),
             dma((3, S)),
             dma((S,)),
             dma((3, S)),
@@ -470,12 +517,13 @@
             dma((L,)),
             dma((L,)),
             dma((L,)),
-            dma((2,)),
-            dma((T - 1,)),
-            dma((T - 1,)),
+            dma((L,)),
+            dma((L,)),
+            dma((L, T - 1)),
+            dma((L, T - 1)),
         ],
         compiler_params=pltpu.CompilerParams(collective_id=0, has_side_effects=True),
-    )(tokens, w, o, query_gain.reshape(1, HEAD_DIM), key_gain.reshape(1, HEAD_DIM))
+    )(tokens, w, v, o, query_gain.reshape(1, HEAD_DIM), key_gain.reshape(1, HEAD_DIM))
 
 
 def solution(mesh):

time: 85.2 us -> 84.3 us (0.989)
  other arithmetic: 0.84 us -> 2.3 us
  local copies, waits for them, and re-layouts: 3.69 us -> 2.64 us
  Pallas kernels: 80.2 us -> 79.2 us
    another operation x2, other arithmetic: 0.84 us -> 2.3 us  [the longest x1 1.57 us: per_device(): v = jnp.stack([key_weight, value_weight])]
    pallas_call x1, Pallas kernels: 80.2 us -> 79.2 us  [per_device(): pl.pallas_call(functools.partial(kernel, S, T), out_shape=jax.ShapeDtypeS...]
    slice x1 -> x0, local copies, waits for them, and re-layouts: 1.02 us -> none  [per_device(): query_weight[:, :hw]]
    unnamed x7 -> x5, local copies, waits for them, and re-layouts: 1.83 us -> 1.8 us
where the time goes in v2:
time: 84.3 us; the launch traced here: 84.1 us
  Pallas kernels  79.2 us (94%)
  local copies, waits for them, and re-layouts  2.64 us (3%)
  other arithmetic  2.3 us (3%)
    pallas_call x1, Pallas kernels, per_device(): pl.pallas_call(functools.partial(kernel, S, T), out_shape=jax.ShapeDtypeS...  79.2 us
    unnamed x5, local copies, waits for them, and re-layouts  1.8 us

profile of v2, /device:TPU:0, one launch (start us, length us, event | category | flops | bytes accessed | tf_op | source)
XLA Modules:
  0.0 84.1 jit_solution(12953840407879853820)
XLA Ops:
  0.0 0.0 copy-start
  0.0 1.6 %pad_maximum_fusion.1.v_ref = bf16[2,256,128]{2,1,0:T(8,128)(2,1)} fusion(bf16[1,256,128]{2,1,0:T(8,128)(2,1)} %bitcast.12, bf16[1,256,128]{2,1,0:T(8,128)(2,1)} %bitcast.13), kind=kLoop, calls=%fused_computation.1 | loop fusion | flops 65536 | bytes 262144 | tf_op jit(solution)/shard_map/stack | solution.py:480
  1.6 0.0 copy-done
  1.6 0.0 copy-start.1
  1.6 0.8 copy.8
  2.4 0.1 copy-done.1
  2.6 0.7 pad_maximum_fusion.w_ref
  3.3 79.2 %shard_map.73 = bf16[64,2048]{1,0:T(8,128)(2,1)} custom-call(bf16[64,2048]{1,0:T(8,128)(2,1)} %x_ref.1, bf16[2,256,256]{2,1,0:T(8,128)(2,1)} %pad_maximum_fusion.w_ref, bf16[2,256,128]{2,1,0:T(8,128)(2,1)} %pad_maximum_fusion.1.v_ref, bf16[2,256,256]{2,1,0:T(8,128)(2,1)} %bitcast.10, f32[1,128]{1,0:T(1,128)} %bitcast.14, f32[1,128]{1,0:T(1,128)} %bitcast.15), custom_call_target="tpu_custom_call" | custom-call | tf_op jit(solution)/shard_map/pallas_call | solution.py:485
  82.5 1.7 %copy.10 = bf16[64,2048]{1,0:T(8,128)(2,1)} copy(bf16[64,2048]{1,0:T(8,128)(2,1)} %shard_map.73) | data formatting | bytes 524288
  (1 shorter events, 0.0 us)
Async XLA Ops:
  0.0 1.6 %copy-start = (bf16[512,256]{1,0:T(8,128)(2,1)S(1)}, bf16[512,256]{1,0:T(8,128)(2,1)}, u32[]{:S(2)}) copy-start(bf16[512,256]{1,0:T(8,128)(2,1)} %param.11) | copy-start | bytes 786436
  1.6 1.0 %copy-start.1 = (bf16[256,512]{1,0:T(8,128)(2,1)S(1)}, bf16[256,512]{1,0:T(8,128)(2,1)}, u32[]{:S(2)}) copy-start(bf16[256,512]{1,0:T(8,128)(2,1)} %param.8) | copy-start | bytes 786436

commit v3 on v2

--- a/solution.py
+++ b/solution.py
@@ -296,9 +296,8 @@
 
         def one(r, _):
             q_at = pl.ds(pl.multiple_of(r * BLOCK, BLOCK), BLOCK)
-            scores = (
-                lax.dot_general(Q[q_at, :], KV[0, at, :], NT, preferred_element_type=jnp.float32)
-                * factor
+            scores = lax.dot_general(
+                Q[q_at, :], KV[0, at, :], NT, preferred_element_type=jnp.float32
             )
             old = best[q_at, :]
             fresh = jnp.maximum(old, jnp.max(scores, axis=-1, keepdims=True))
@@ -311,16 +310,16 @@
             )
             return 0
 
-        lax.fori_loop(0, heads * M // BLOCK, one, 0)
-
-    def attend_at(d):
+        lax.fori_loop(0, heads * M // BLOCK, one, 0, unroll=True)
+
+    def both_ways(act, d):
         @pl.when(line >= d)
         def _():
-            attend(line - d)
+            act(line - d)
 
         @pl.when(line + d < L)
         def _():
-            attend(line + d)
+            act(line + d)
 
     kv_push(line, 0)
     kv_push(line, 1)
@@ -331,10 +330,11 @@
         weights.step(d)
         return 0
 
-    lax.fori_loop(2, L, weight_step, 0)
-    kv_step(L - 1)
+    lax.fori_loop(2, L - 1, weight_step, 0)
+    kv_step(L - 2)
     outs.push_own()
     outs.push_pair()
+    weights.step(L - 1)
     weights.local().wait()
     outs.local().wait()
     for rb in range(M // BLOCK):
@@ -342,16 +342,19 @@
         raw = jnp.dot(X[at, :], W[...], preferred_element_type=jnp.float32).astype(jnp.bfloat16)
         for j in range(heads):
             part = raw[:, j * HEAD_DIM : (j + 1) * HEAD_DIM].astype(jnp.float32)
-            Q[pl.ds(j * M + rb * BLOCK, BLOCK), :] = turned(part, qg_ref[...], at)
+            Q[pl.ds(j * M + rb * BLOCK, BLOCK), :] = turned(part, qg_ref[...] * factor, at)
 
     attend(line)
+    both_ways(attend, 1)
     outs.step(1)
 
     def attend_round(d, _):
-        attend_at(d)
+        both_ways(attend, d)
         return 0
 
-    lax.fori_loop(1, L, attend_round, 0)
+    lax.fori_loop(2, L - 1, attend_round, 0)
+    kv_step(L - 1)
+    both_ways(attend, L - 1)
 
     for ph in range(2):
         for pt in range(T):
@@ -398,15 +401,6 @@
         for i in range(1, T):
             SF[g, i - 1] = reduced(g, lax.rem(h + i, T)).astype(jnp.bfloat16)
             final_send(g, i).start()
-
-    def both_ways(act, d):
-        @pl.when(line >= d)
-        def _():
-            act(line - d)
-
-        @pl.when(line + d < L)
-        def _():
-            act(line + d)
 
     multiply(line)
     both_ways(multiply, 1)

time: 84.3 us -> 83.9 us (level)
  no operation moved by 1% of the time
where the time goes in v3:
time: 83.9 us; the launch traced here: 83.6 us
  Pallas kernels  78.7 us (94%)
  local copies, waits for them, and re-layouts  2.64 us (3%)
  other arithmetic  2.3 us (3%)
    pallas_call x1, Pallas kernels, per_device(): pl.pallas_call(functools.partial(kernel, S, T), out_shape=jax.ShapeDtypeS...  78.7 us
    unnamed x5, local copies, waits for them, and re-layouts  1.8 us

profile of v3, /device:TPU:0, one launch (start us, length us, event | category | flops | bytes accessed | tf_op | source)
XLA Modules:
  0.0 83.6 jit_solution(15715031555447631305)
XLA Ops:
  0.0 0.0 copy-start
  0.0 1.6 %pad_maximum_fusion.1.v_ref = bf16[2,256,128]{2,1,0:T(8,128)(2,1)} fusion(bf16[1,256,128]{2,1,0:T(8,128)(2,1)} %bitcast.12, bf16[1,256,128]{2,1,0:T(8,128)(2,1)} %bitcast.13), kind=kLoop, calls=%fused_computation.1 | loop fusion | flops 65536 | bytes 262144 | tf_op jit(solution)/shard_map/stack | solution.py:474
  1.6 0.0 copy-done
  1.6 0.0 copy-start.1
  1.6 0.8 copy.8
  2.4 0.1 copy-done.1
  2.6 0.7 pad_maximum_fusion.w_ref
  3.3 78.7 %shard_map.73 = bf16[64,2048]{1,0:T(8,128)(2,1)} custom-call(bf16[64,2048]{1,0:T(8,128)(2,1)} %x_ref.1, bf16[2,256,256]{2,1,0:T(8,128)(2,1)} %pad_maximum_fusion.w_ref, bf16[2,256,128]{2,1,0:T(8,128)(2,1)} %pad_maximum_fusion.1.v_ref, bf16[2,256,256]{2,1,0:T(8,128)(2,1)} %bitcast.10, f32[1,128]{1,0:T(1,128)} %bitcast.14, f32[1,128]{1,0:T(1,128)} %bitcast.15), custom_call_target="tpu_custom_call" | custom-call | tf_op jit(solution)/shard_map/pallas_call | solution.py:479
  82.0 1.7 %copy.10 = bf16[64,2048]{1,0:T(8,128)(2,1)} copy(bf16[64,2048]{1,0:T(8,128)(2,1)} %shard_map.73) | data formatting | bytes 524288
  (1 shorter events, 0.0 us)
Async XLA Ops:
  0.0 1.6 %copy-start = (bf16[512,256]{1,0:T(8,128)(2,1)S(1)}, bf16[512,256]{1,0:T(8,128)(2,1)}, u32[]{:S(2)}) copy-start(bf16[512,256]{1,0:T(8,128)(2,1)} %param.11) | copy-start | bytes 786436
  1.6 1.0 %copy-start.1 = (bf16[256,512]{1,0:T(8,128)(2,1)S(1)}, bf16[256,512]{1,0:T(8,128)(2,1)}, u32[]{:S(2)}) copy-start(bf16[256,512]{1,0:T(8,128)(2,1)} %param.8) | copy-start | bytes 786436

commit v4 on v3

--- a/solution.py
+++ b/solution.py
@@ -53,23 +53,44 @@
         def _():
             self.along(source, way, src).start()
 
-    def pair(self):
+    def each(self, which, act):
+        if isinstance(self.own, tuple):
+            for k, ref in enumerate(self.own):
+
+                @pl.when(which == k)
+                def _():
+                    act(ref)
+
+        else:
+            act(self.own(which))
+
+    def any_own(self):
+        return self.own[0] if isinstance(self.own, tuple) else self.own(0)
+
+    def pair(self, src=None):
         return remote(
-            self.own.at[1 - self.half],
+            self.any_own() if src is None else src,
             self.place(self.s),
             self.send.at[2, self.s],
             self.recv.at[self.s],
             (self.s + 1 - 2 * self.half, self.t),
         )
 
-    def local(self):
+    def local(self, src=None):
         return pltpu.make_async_copy(
-            self.own.at[self.half], self.place(self.s), self.send.at[2, self.s + 1 - 2 * self.half]
-        )
+            self.any_own() if src is None else src,
+            self.place(self.s),
+            self.send.at[2, self.s + 1 - 2 * self.half],
+        )
+
+    def push_pair_own(self):
+        self.each(1 - self.half, lambda src: self.pair(src).start())
+
+    def keep_own(self):
+        self.each(self.half, lambda src: self.local(src).start())
 
     def push_own(self):
-        self.push(self.s, 0, self.own.at[self.half])
-        self.push(self.s, 1, self.own.at[self.half])
+        self.each(self.half, lambda src: (self.push(self.s, 0, src), self.push(self.s, 1, src)))
 
     def arrived(self, source):
         self.along(source, 0).wait_recv()
@@ -113,16 +134,16 @@
 
 def kernel(
     S, T,
-    x_ref, w_ref, v_ref, o_ref, qg_ref, kg_ref, out_ref,
-    X, W, WV, OW, KV, Q, A, C, SN, best, total, summed, PS, SB, RC, SF, RF,
+    x_ref, w_ref, k_ref, v_ref, o_ref, qg_ref, kg_ref, out_ref,
+    X, W, WV, OT, OW, KV, Q, A, C, SN, best, total, summed, PS, SB, RC, SF, RF,
     xs_sem, xr_sem, ws_sem, wr_sem, vs_sem, vr_sem, os_sem, or_sem, ks_sem, kr_sem, kp_sem, kq_sem,
     cs_sem, cr_sem, fs_sem, fr_sem,
 ):
     L, N = S // 2, 2 * T
     R, D = x_ref.shape
     M = N * R
-    wr = w_ref.shape[1]
-    oc, hw = o_ref.shape[1:]
+    wr = w_ref.shape[0]
+    hw, oc = o_ref.shape[0] // 2, o_ref.shape[1]
     heads = hw // HEAD_DIM
     s, t = lax.axis_index("sp"), lax.axis_index("tp")
     line, half = s // 2, lax.rem(s, 2)
@@ -155,9 +176,9 @@
         N - 1 + jnp.where(line > 0, 1, 0) + jnp.where(line < L - 1, 1, 0),
     )
 
-    weights = Line(w_ref, W, wr, ws_sem, wr_sem, s, t, L)
-    kv_weights = Line(v_ref, WV, wr, vs_sem, vr_sem, s, t, L)
-    outs = Line(o_ref, OW, oc, os_sem, or_sem, s, t, L)
+    weights = Line(lambda k: w_ref.at[:, pl.ds(pl.multiple_of(k * hw, hw), hw)], W, wr, ws_sem, wr_sem, s, t, L)
+    kv_weights = Line((k_ref, v_ref), WV, wr, vs_sem, vr_sem, s, t, L)
+    outs = Line(lambda k: OT.at[k], OW, oc, os_sem, or_sem, s, t, L)
 
     def rows(b):
         return X.at[pl.ds(pl.multiple_of(b * R, R), R)]
@@ -179,16 +200,16 @@
             x_ref if i == 0 else rows(b), rows(b), xs_sem.at[T + i], xr_sem.at[b], (s, mate)
         )
 
-    kv_weights.pair().start()
+    kv_weights.push_pair_own()
     kv_weights.push_own()
-    weights.pair().start()
+    weights.push_pair_own()
     for i in range(1, T):
         token_send(i).start()
     token_mate(0).start()
-    outs.pair().start()
-    kv_weights.local().start()
-    weights.local().start()
-    outs.local().start()
+    for k in range(2):
+        OT[k] = o_ref[k * hw : (k + 1) * hw, :].T
+    kv_weights.keep_own()
+    weights.keep_own()
     own_tokens = pltpu.make_async_copy(x_ref, rows(slot), xs_sem.at[0])
     own_tokens.start()
 
@@ -212,6 +233,8 @@
     total[...] = jnp.zeros_like(total)
     summed[...] = jnp.zeros_like(summed)
 
+    outs.push_pair_own()
+    outs.keep_own()
     kv_weights.push_pair()
 
     def kv_weight_step(d, _):
@@ -470,21 +493,19 @@
     hw = query_weight.shape[1] // 2
     heads = hw // HEAD_DIM
     wr, oc = query_weight.shape[0], out_weight.shape[1]
-    w = jnp.stack([query_weight[:, :hw], query_weight[:, hw:]])
-    v = jnp.stack([key_weight, value_weight])
-    o = jnp.swapaxes(out_weight.reshape(2, hw, oc), 1, 2)
     vmem = pl.BlockSpec(memory_space=pltpu.VMEM)
     bf, f32 = jnp.bfloat16, jnp.float32
     dma = pltpu.SemaphoreType.DMA
     return pl.pallas_call(
         functools.partial(kernel, S, T),
         out_shape=jax.ShapeDtypeStruct((R, D), bf),
-        in_specs=[vmem] * 6,
+        in_specs=[vmem] * 7,
         out_specs=vmem,
         scratch_shapes=[
             pltpu.VMEM((M, D), bf),
             pltpu.VMEM((S * wr, hw), bf),
             pltpu.VMEM((S * wr, HEAD_DIM), bf),
+            pltpu.VMEM((2, oc, hw), bf),
             pltpu.VMEM((S * oc, hw), bf),
             pltpu.VMEM((2, L * M, HEAD_DIM), bf),
             pltpu.VMEM((heads * M, HEAD_DIM), bf),
@@ -517,7 +538,10 @@
             dma((L, T - 1)),
         ],
         compiler_params=pltpu.CompilerParams(collective_id=0, has_side_effects=True),
-    )(tokens, w, v, o, query_gain.reshape(1, HEAD_DIM), key_gain.reshape(1, HEAD_DIM))
+    )(
+        tokens, query_weight, key_weight, value_weight, out_weight,
+        query_gain.reshape(1, HEAD_DIM), key_gain.reshape(1, HEAD_DIM),
+    )
 
 
 def solution(mesh):

time: 83.9 us -> 80.6 us (0.961)
  other arithmetic: 2.3 us -> 0 us
  local copies, waits for them, and re-layouts: 2.64 us -> 1.67 us
    another operation x2 -> x0, other arithmetic: 2.3 us -> none  [the longest x1 1.57 us: per_device(): v = jnp.stack([key_weight, value_weight])]
    unnamed x5 -> x1, local copies, waits for them, and re-layouts: 1.8 us -> 1.67 us
where the time goes in v4:
time: 80.6 us; the launch traced here: 80.4 us
  Pallas kernels  78.7 us (98%)
  local copies, waits for them, and re-layouts  1.67 us (2%)
    pallas_call x1, Pallas kernels, per_device(): pl.pallas_call(functools.partial(kernel, S, T), out_shape=jax.ShapeDtypeS...  78.7 us
    unnamed x1, local copies, waits for them, and re-layouts  1.67 us

profile of v4, /device:TPU:0, one launch (start us, length us, event | category | flops | bytes accessed | tf_op | source)
XLA Modules:
  0.0 80.4 jit_solution(14918646763154917947)
XLA Ops:
  0.0 78.7 %shard_map.73 = bf16[64,2048]{1,0:T(8,128)(2,1)} custom-call(bf16[64,2048]{1,0:T(8,128)(2,1)} %x_ref.1, bf16[256,512]{1,0:T(8,128)(2,1)} %w_ref.1, bf16[256,128]{1,0:T(8,128)(2,1)} %k_ref.1, bf16[256,128]{1,0:T(8,128)(2,1)} %v_ref.1, bf16[512,256]{1,0:T(8,128)(2,1)} %o_ref.1, f32[1,128]{1,0:T(1,128)} %bitcast.2, f32[1,128]{1,0:T(1,128)} %bitcast.3), custom_call_target="tpu_custom_call" | custom-call | tf_op jit(solution)/shard_map/pallas_call | solution.py:499
  78.7 1.7 %copy.9 = bf16[64,2048]{1,0:T(8,128)(2,1)} copy(bf16[64,2048]{1,0:T(8,128)(2,1)} %shard_map.73) | data formatting | bytes 524288

commit v5 on v4

--- a/solution.py
+++ b/solution.py
@@ -367,9 +367,18 @@
             part = raw[:, j * HEAD_DIM : (j + 1) * HEAD_DIM].astype(jnp.float32)
             Q[pl.ds(j * M + rb * BLOCK, BLOCK), :] = turned(part, qg_ref[...] * factor, at)
 
+    inner = (line > 0) & (line < L - 1)
     attend(line)
+    outs.step(1)
     both_ways(attend, 1)
-    outs.step(1)
+
+    @pl.when(inner)
+    def _():
+        def relay(d, _):
+            outs.step(d)
+            return 0
+
+        lax.fori_loop(2, L, relay, 0)
 
     def attend_round(d, _):
         both_ways(attend, d)
@@ -431,7 +440,11 @@
 
     def out_round(d, _):
         both_ways(spread, d - 1)
-        outs.step(d)
+
+        @pl.when(jnp.logical_not(inner))
+        def _():
+            outs.step(d)
+
         both_ways(multiply, d)
         return 0
 

time: 80.6 us -> 82.4 us (1.022)
  Pallas kernels: 78.7 us -> 80.5 us
    pallas_call x1, Pallas kernels: 78.7 us -> 80.5 us  [per_device(): pl.pallas_call(functools.partial(kernel, S, T), out_shape=jax.ShapeDtypeS...]
where the time goes in v5:
time: 82.4 us; the launch traced here: 82.2 us
  Pallas kernels  80.5 us (98%)
  local copies, waits for them, and re-layouts  1.67 us (2%)
    pallas_call x1, Pallas kernels, per_device(): pl.pallas_call(functools.partial(kernel, S, T), out_shape=jax.ShapeDtypeS...  80.5 us
    unnamed x1, local copies, waits for them, and re-layouts  1.67 us

profile of v5, /device:TPU:0, one launch (start us, length us, event | category | flops | bytes accessed | tf_op | source)
XLA Modules:
  0.0 82.2 jit_solution(9392846397222555140)
XLA Ops:
  0.0 80.5 %shard_map.73 = bf16[64,2048]{1,0:T(8,128)(2,1)} custom-call(bf16[64,2048]{1,0:T(8,128)(2,1)} %x_ref.1, bf16[256,512]{1,0:T(8,128)(2,1)} %w_ref.1, bf16[256,128]{1,0:T(8,128)(2,1)} %k_ref.1, bf16[256,128]{1,0:T(8,128)(2,1)} %v_ref.1, bf16[512,256]{1,0:T(8,128)(2,1)} %o_ref.1, f32[1,128]{1,0:T(1,128)} %bitcast.2, f32[1,128]{1,0:T(1,128)} %bitcast.3), custom_call_target="tpu_custom_call" | custom-call | tf_op jit(solution)/shard_map/pallas_call | solution.py:512
  80.5 1.7 %copy.9 = bf16[64,2048]{1,0:T(8,128)(2,1)} copy(bf16[64,2048]{1,0:T(8,128)(2,1)} %shard_map.73) | data formatting | bytes 524288
